TPU v7x, 32 devices: a whole 2x2x4 slice. The times are simulated.
32 devices in a mesh: sp: 16 (over z, y, x), tp: 2 (over core).
Axes of the slice: x: 2, y: 2, z: 4, core: 2. Of those that a mesh axis runs over, the one named last changes fastest.
Arguments:
- query_logits: bfloat16 [2048, 1024], P('sp', 'tp'), may hold values from -6 to 6
- value_rows: bfloat16 [2048, 1024], P('sp', 'tp'), may hold values from -6 to 6
- onward_forget_logits: bfloat16 [2048, 1024], P('sp', 'tp'), may hold values from -5.5 to 5.5
- reverse_forget_logits: bfloat16 [2048, 1024], P('sp', 'tp'), may hold values from -5.5 to 5.5
- output_gate_logits: bfloat16 [2048, 1024], P('sp', 'tp'), may hold values from -6 to 6
- onward_floor_gap: float32 [1024], P('tp'), may hold values from 0 to 0.12, as said below
- reverse_floor_gap: float32 [1024], P('tp'), may hold values from 0 to 0.12, as said below
- extra_log_decay: float32 [2048, 8], P('sp', 'tp'), may hold values from -2.1 to 0
- per_head_gain: float32 [128], replicated, may hold values from 0.1 to 1.9
- residual: bfloat16 [2048, 2048], P('sp', 'tp'), may hold values from -8 to 8
- output_matrix: bfloat16 [1024, 2048], P(None, 'tp'), may hold values from -0.375 to 0.375
- inner_norm_gain: float32 [2048], P('tp'), may hold values from 0.1 to 1.9
- inner_norm_bias: float32 [2048], P('tp'), may hold values from -1.5 to 1.5
- gate_matrix: bfloat16 [2048, 5632], P('sp', 'tp'), may hold values from -0.125 to 0.125
- up_matrix: bfloat16 [2048, 5632], P('sp', 'tp'), may hold values from -0.125 to 0.125
- down_matrix: bfloat16 [5632, 2048], P('tp', 'sp'), may hold values from -0.15625 to 0.15625
- closing_norm_gain: float32 [2048], P('tp'), may hold values from 0.1 to 1.9
- closing_norm_bias: float32 [2048], P('tp'), may hold values from -1.5 to 1.5
Outputs:
- layer_output: bfloat16 [2048, 2048], P('sp', 'tp')
Inputs may be any that keep to these rules, and one draw needn't show every extreme that they name: `onward_floor_gap`: positive. `reverse_floor_gap`: positive.
All inputs are finite; a program needn't handle non-finite values.
Results may differ from a plain program's by a relative error of at most 0.014.
Values may be sent and summed in bfloat16 or wider, within the bound.
A program may use at most 128 MiB of HBM per device.

v0:
```python
import math
import jax
import jax.numpy as jnp
from jax import lax
from jax.sharding import PartitionSpec as P

D = 2048
highest_precision = lax.Precision.HIGHEST
alpha_mix = 2.0**0.25
norm_eps = 1e-05
head_eps = 1e-06


def prefix(x, axis, join, neutral, backward):
    count = lax.axis_size(axis)
    place = lax.axis_index(axis)
    ahead = count - 1 - place if backward else place
    gathered = jax.tree.map(
        lambda a, kind: lax.all_gather(a.astype(kind), axis), x, (jnp.bfloat16, jnp.bfloat16)
    )
    state = jax.tree.map(lambda a, e: jnp.zeros_like(a) + jnp.asarray(e, a.dtype), x, neutral)

    def one(step, state):
        source = count - 1 - step if backward else step
        return join(
            state,
            jax.tree.map(
                lambda a, own: lax.dynamic_index_in_dim(a, source, 0, False).astype(own.dtype),
                gathered,
                x,
            ),
        )

    return lax.fori_loop(0, ahead, one, state)


def decay_factors(unscaled_input, lower_bound_gap, extra_decays):
    decay_factor = lower_bound_gap * jax.nn.sigmoid(-unscaled_input.astype(jnp.float32))
    return (jnp.log1p(-decay_factor) + extra_decays, decay_factor)


def local_pass(query, keys, values, log_decay):
    rows, head_count, model_width = query.shape
    span = math.gcd(rows, 128)
    count = rows // span
    triangle = jnp.tril(jnp.ones((span, span), jnp.float32))

    def blocks(array):
        return array.reshape(count, span, head_count, array.shape[2])

    def advance(carry, inputs):
        running_state, offset = carry
        query_block, key_block, value_tile, log_block = inputs
        running = jnp.cumsum(log_block, axis=0)
        final_index = running[-1]
        decayed_query = query_block * jnp.exp(running)
        key_inverse = key_block * jnp.exp(-running)
        key_stop = key_block * jnp.exp(final_index[None] - running)
        scores = (
            jnp.einsum("thk,shk->hts", decayed_query, key_inverse, precision=highest_precision)
            * triangle[None]
        )
        inner = jnp.einsum("hts,shv->thv", scores, value_tile, precision=highest_precision)
        carried_state = jnp.einsum(
            "nex,exl->nel", decayed_query, running_state, precision=highest_precision
        )
        query_start = decayed_query * jnp.exp(offset)[None]
        running_state = jnp.exp(final_index)[:, :, None] * running_state + jnp.einsum(
            "ojy,oje->jye", key_stop, value_tile, precision=highest_precision
        )
        return ((running_state, offset + final_index), (inner + carried_state, query_start))

    start = (
        jnp.zeros((head_count, model_width, values.shape[2]), jnp.float32),
        jnp.zeros((head_count, model_width), jnp.float32),
    )
    final, outputs = lax.scan(
        advance, start, (blocks(query), blocks(keys), blocks(values), blocks(log_decay))
    )
    result = outputs[0].reshape(rows, head_count, values.shape[2])
    query_start = outputs[1].reshape(rows, head_count, model_width)
    return (result, query_start, final[1], final[0])


def join(earlier, later):
    return (earlier[0] + later[0], jnp.exp(later[0])[:, :, None] * earlier[1] + later[1])


def row_norm(before, moments, gain, bias):
    mean = moments[0] / D
    spread = moments[1] / D - mean * mean
    return (before - mean[:, None]) * lax.rsqrt(spread + norm_eps)[:, None] * gain + bias


def shards(
    query_logits,
    value_rows,
    onward_forget_logits,
    reverse_forget_logits,
    output_gate_logits,
    onward_floor_gap,
    reverse_floor_gap,
    extra_log_decay,
    per_head_gain,
    residual,
    output_matrix,
    inner_norm_gain,
    inner_norm_bias,
    gate_matrix,
    up_matrix,
    down_matrix,
    closing_norm_gain,
    closing_norm_bias,
):
    gate_whole, up_whole, down_whole = (
        lax.all_gather(gate_matrix, "sp", axis=0, tiled=True),
        lax.all_gather(up_matrix, "sp", axis=0, tiled=True),
        lax.all_gather(down_matrix, "sp", axis=1, tiled=True),
    )
    rows = query_logits.shape[0]
    head_count = extra_log_decay.shape[1]
    model_width = query_logits.shape[1] // head_count
    shape_head = (rows, head_count, model_width)
    query = jax.nn.silu(query_logits.astype(jnp.float32)).reshape(shape_head)
    values = value_rows.astype(jnp.float32).reshape(shape_head)
    extra_decays = jnp.repeat(extra_log_decay, model_width, axis=1)
    onward_log_decay, onward_key_rows = decay_factors(
        onward_forget_logits, onward_floor_gap, extra_decays
    )
    reverse_log_decay, reverse_key_rows = decay_factors(
        reverse_forget_logits, reverse_floor_gap, extra_decays
    )
    empty_total = jnp.zeros((head_count, model_width), jnp.float32)
    empty_state = jnp.zeros((head_count, model_width, model_width), jnp.float32)
    upcoming_part, upcoming_begin, ahead_total, ahead_state = local_pass(
        query, onward_key_rows.reshape(shape_head), values, onward_log_decay.reshape(shape_head)
    )
    incoming_state = prefix(
        (ahead_total, ahead_state), "sp", join, (empty_total, empty_state), False
    )
    upcoming_part = upcoming_part + jnp.einsum(
        "nex,exl->nel", upcoming_begin, incoming_state[1], precision=highest_precision
    )
    preceding_part, preceding_begin, behind_total, behind_state = local_pass(
        jnp.flip(query, axis=0),
        jnp.flip(reverse_key_rows.reshape(shape_head), axis=0),
        jnp.flip(values, axis=0),
        jnp.flip(reverse_log_decay.reshape(shape_head), axis=0),
    )
    arriving_state = prefix(
        (behind_total, behind_state), "sp", join, (empty_total, empty_state), True
    )
    preceding_part = jnp.flip(
        preceding_part
        + jnp.einsum(
            "nex,exl->nel", preceding_begin, arriving_state[1], precision=highest_precision
        ),
        axis=0,
    )
    mixed = upcoming_part + preceding_part
    normed = (
        mixed * lax.rsqrt(jnp.mean(mixed * mixed, axis=2, keepdims=True) + head_eps) * per_head_gain
    )
    gated = (
        normed.reshape(rows, head_count * model_width)
        * jax.nn.silu(output_gate_logits.astype(jnp.float32))
    ).astype(jnp.bfloat16)
    mixer = jnp.dot(
        lax.all_gather(gated, "tp", axis=1, tiled=True),
        output_matrix,
        preferred_element_type=jnp.float32,
    )
    before_middle = alpha_mix * residual.astype(jnp.float32) + mixer
    moments = lax.psum(
        (jnp.sum(before_middle, axis=1), jnp.sum(before_middle * before_middle, axis=1)), "tp"
    )
    middle = row_norm(before_middle, moments, inner_norm_gain, inner_norm_bias).astype(jnp.bfloat16)
    whole = lax.all_gather(middle, "tp", axis=1, tiled=True)
    gate = jnp.dot(whole, gate_whole, preferred_element_type=jnp.float32)
    up = jnp.dot(whole, up_whole, preferred_element_type=jnp.float32)
    hidden = (jax.nn.silu(gate) * up).astype(jnp.bfloat16)
    partial_value = jnp.dot(hidden, down_whole, preferred_element_type=jnp.float32)
    feed = lax.psum_scatter(
        partial_value.astype(jnp.bfloat16), "tp", scatter_dimension=1, tiled=True
    ).astype(jnp.float32)
    before_final = alpha_mix * middle.astype(jnp.float32) + feed
    closing = lax.psum(
        (jnp.sum(before_final, axis=1), jnp.sum(before_final * before_final, axis=1)), "tp"
    )
    return row_norm(before_final, closing, closing_norm_gain, closing_norm_bias).astype(
        jnp.bfloat16
    )


def solution(mesh):
    placed = (
        P("sp", "tp"),
        P("sp", "tp"),
        P("sp", "tp"),
        P("sp", "tp"),
        P("sp", "tp"),
        P("tp"),
        P("tp"),
        P("sp", "tp"),
        P(),
        P("sp", "tp"),
        P(None, "tp"),
        P("tp"),
        P("tp"),
        P("sp", "tp"),
        P("sp", "tp"),
        P("tp", "sp"),
        P("tp"),
        P("tp"),
    )
    return jax.shard_map(
        shards, mesh=mesh, in_specs=placed, out_specs=P("sp", "tp"), check_vma=False
    )
```

profile of v0, /device:TPU:0, one launch (start us, length us, event | category | flops | bytes accessed | tf_op | source)
XLA Modules:
  0.0 643.3 jit_solution(78488061301699797)
XLA Ops:
  6.5 0.9 copy.35
  7.7 2.1 bitcast_add_fusion.1
  10.3 1.7 reshape.106
  12.1 0.8 squeeze.50
  12.8 1.0 convert_multiply_fusion.1
  13.8 0.8 squeeze.48
  14.8 2.4 exponential_multiply_fusion.3
  17.2 1.3 fusion.7
  18.6 2.0 fusion.6
  22.6 44.0 %all_gather.38 = bf16[16,4,128]{2,1,0:T(4,128)(2,1)} all-gather(bf16[1,4,128]{2,1,0:T(4,128)(2,1)S(1)} %slice.20), channel_id=1, replica_groups=mesh['sp'=16,'tp'=2] {'sp'}, dimensions={0}, use_global_device_ids=true | all-gather | bytes 17408 | tf_op jit(solution)/shard_map/all_gather | solution.py:19
  66.7 35.8 %all_gather.35 = bf16[16,4,128]{2,1,0:T(4,128)(2,1)S(1)} all-gather(bf16[1,4,128]{2,1,0:T(4,128)(2,1)S(1)} %slice.21), channel_id=1, replica_groups=mesh['sp'=16,'tp'=2] {'sp'}, dimensions={0}, use_global_device_ids=true | all-gather | bytes 17408 | tf_op jit(solution)/shard_map/all_gather | solution.py:19
  102.5 1.6 convolution_multiply_fusion.2
  107.2 26.5 %while.17 = (s32[]{:T(128)}, f32[4,128,128]{2,1,0:T(8,128)S(1)}, s32[]{:T(128)}, bf16[16,4,128]{2,1,0:T(4,128)(2,1)}, bf16[16,4,128,128]{3,2,1,0:T(8,128)(2,1)},...) while((s32[]{:T(128)}, f32[4,128,128]{2,1,0:T(8,128)S(1)}, s32[]{:T(128)}, bf16[16,4,128]{2,1,0:T(4,128)(2,1)}, ...), condition=%wide.region_5.6_spmd, body=%wide.region_4.5_spmd.sunk | while | flops 197126 | bytes 660627 | solution.py:34
  107.8 1.1 convert_add_fusion.6
  109.6 1.1 convert_add_fusion.6
  110.7 0.7 exponential_bitcast_fusion.5
  111.4 1.1 convert_add_fusion.6
  113.1 1.1 convert_add_fusion.6
  114.8 1.1 convert_add_fusion.6
  116.6 1.1 convert_add_fusion.6
  118.3 1.1 convert_add_fusion.6
  119.4 0.7 exponential_bitcast_fusion.5
  120.1 1.1 convert_add_fusion.6
  121.9 1.1 convert_add_fusion.6
  123.0 0.7 exponential_bitcast_fusion.5
  123.7 1.1 convert_add_fusion.6
  125.5 1.1 convert_add_fusion.6
  127.2 1.1 convert_add_fusion.6
  129.0 1.1 convert_add_fusion.6
  130.1 0.7 exponential_bitcast_fusion.5
  130.8 1.1 convert_add_fusion.6
  132.5 1.1 convert_add_fusion.6
  133.6 1.3 fusion.1
  134.9 1.9 rev.20
  136.9 7.2 %all-gather.14.cloned.1.call-done = bf16[64,128,128]{2,1,0:T(8,128)(2,1)} async-done(((bf16[4,128,128]{2,1,0:T(8,128)(2,1)}), bf16[64,128,128]{2,1,0:T(8,128)(2,1)}) %all-gather.14.cloned.1.call-update) | async-done | bytes 2097168 | tf_op jit(solution)/shard_map/all_gather | solution.py:19
  144.7 0.7 multiply_multiply_fusion
  145.7 2.0 all_gather.41
  148.3 2.5 all-reduce.1
  151.0 2.4 all_gather.42
  153.3 133.7 %all-gather.8.cloned.1.call-done = bf16[2048,2816]{1,0:T(8,128)(2,1)} async-done(((bf16[128,2816]{1,0:T(8,128)(2,1)}), bf16[2048,2816]{1,0:T(8,128)(2,1)}) %all-gather.8.cloned.1.call-update) | async-done | bytes 11534352 | tf_op jit(solution)/shard_map/all_gather | solution.py:116
  287.0 7.0 %fusion.40 = f32[128,2816]{1,0:T(8,128)} fusion(bf16[128,2048]{1,0:T(8,128)(2,1)S(1)} %all_gather.42, bf16[2048,2816]{1,0:T(8,128)(2,1)} %all-gather.8.cloned.1.call-done), kind=kOutput, calls=%fused_computation.91 | convolution fusion | flops 1476395008 | bytes 13500416 | tf_op jit(solution)/shard_map/dot_general | solution.py:179
  294.1 135.2 %all-gather.10.cloned.1.call-done = bf16[2048,2816]{1,0:T(8,128)(2,1)} async-done(((bf16[128,2816]{1,0:T(8,128)(2,1)}), bf16[2048,2816]{1,0:T(8,128)(2,1)}) %all-gather.10.cloned.1.call-update) | async-done | bytes 11534352 | tf_op jit(solution)/shard_map/all_gather | solution.py:117
  429.3 182.8 %all-gather.12.cloned.1.call-done = bf16[2816,2048]{1,0:T(8,128)(2,1)} async-done(((bf16[2816,128]{1,0:T(8,128)(2,1)}), bf16[2816,2048]{1,0:T(8,128)(2,1)}) %all-gather.12.cloned.1.call-update) | async-done | bytes 11534352 | tf_op jit(solution)/shard_map/all_gather | solution.py:118
  612.1 12.3 %convolution_convert_fusion = bf16[128,2048]{1,0:T(8,128)(2,1)} fusion(bf16[2816,2048]{1,0:T(8,128)(2,1)} %all-gather.12.cloned.1.call-done, bf16[128,2048]{1,0:T(8,128)(2,1)S(1)} %all_gather.42, bf16[2048,2816]{1,0:T(8,128)(2,1)} %all-gather.10.cloned.1.call-done, f32[128,2816]{1,0:T(8,128)} %fusion.40), kind=kOutput, calls=%fused_computation.6 | convolution fusion | flops 2955214848 | bytes 25559040 | tf_op jit(solution)/shard_map/dot_general | solution.py:182
  624.4 6.3 reduce-scatter.2.cloned.1.call-done
  630.7 1.3 fusion.8
  632.0 2.5 all-reduce
  634.5 1.9 add_convert_fusion
  (74 shorter events, 14.7 us)
Async XLA Ops:
  6.5 141.2 %copy-start = (bf16[1024,1024]{1,0:T(8,128)(2,1)S(1)}, bf16[1024,1024]{1,0:T(8,128)(2,1)}, u32[]{:S(2)}) copy-start(bf16[1024,1024]{1,0:T(8,128)(2,1)} %param.32) | copy-start | bytes 6291460
  6.5 100.6 %all-gather.16.cloned.1.call-start = ((), (), s32[]{:S(2)}) async-start(), calls=%async_computation.6 | async-start | bytes 2228224 | tf_op jit(solution)/shard_map/all_gather | solution.py:19
  9.8 4.8 copy-start.1
  9.9 2.1 copy-start.2
  18.5 125.5 %all-gather.14.cloned.1.call-start = ((), (), s32[]{:S(2)}) async-start(), calls=%async_computation.5 | async-start | bytes 2228224 | tf_op jit(solution)/shard_map/all_gather | solution.py:19
  20.6 266.4 %all-gather.8.cloned.1.call-start = ((), (), s32[]{:S(2)}) async-start(), calls=%async_computation.1 | async-start | bytes 12255232 | tf_op jit(solution)/shard_map/all_gather | solution.py:116
  21.4 407.9 %all-gather.10.cloned.1.call-start = ((), (), s32[]{:S(2)}) async-start(), calls=%async_computation.2 | async-start | bytes 12255232 | tf_op jit(solution)/shard_map/all_gather | solution.py:117
  22.0 590.1 %all-gather.12.cloned.1.call-start = ((), (), s32[]{:S(2)}) async-start(), calls=%async_computation.3 | async-start | bytes 12255232 | tf_op jit(solution)/shard_map/all_gather | solution.py:118
  22.5 608.2 %reduce-scatter.2.cloned.1.call-start = ((), (), s32[]{:S(2)}) async-start(), calls=%async_computation.4 | async-start | bytes 786432 | tf_op jit(solution)/shard_map/reduce_scatter | solution.py:183
  22.6 82.6 %copy-start.3 = (f32[128,4,128]{2,1,0:T(4,128)S(1)}, f32[128,4,128]{2,1,0:T(4,128)}, u32[]{:S(2)}) copy-start(f32[128,4,128]{2,1,0:T(4,128)} %get-tuple-element.229) | copy-start | bytes 786436
  144.1 1.5 copy-start.5
  144.1 3.7 copy-start.4
  145.6 5.2 copy-start.6
  145.6 5.2 copy-start.7
  294.1 340.4 %copy-start.8 = (f32[1024]{0:T(1024)S(1)}, f32[1024]{0:T(1024)}, u32[]{:S(2)}) copy-start(f32[1024]{0:T(1024)} %param.39) | copy-start | bytes 12292
  294.1 340.4 %copy-start.9 = (f32[1024]{0:T(1024)S(1)}, f32[1024]{0:T(1024)}, u32[]{:S(2)}) copy-start(f32[1024]{0:T(1024)} %param.38) | copy-start | bytes 12292
Sparse Core Ops, SparseCore 0:
  18.7 63.2 all-gather.15
  84.7 59.2 all-gather.13
  146.8 140.2 all-gather.7
  289.7 139.5 all-gather.9
  431.8 180.2 all-gather.11
  624.5 6.1 reduce-scatter.1
where the time goes:
time: 644 us; the launch traced here: 643 us
  waiting for transfers between devices  467 us (73%)
  blocking collectives  89.1 us (14%)
  other arithmetic  36 us (6%)
  matrix products  29.8 us (5%)
  between operations  13.7 us (2%)
  local copies, waits for them, and re-layouts  6.96 us (1%)
    all_gather x1, waiting for transfers between devices, shards(): lax.all_gather(down_matrix, 'sp', axis=1, tiled=True)  183 us
    all_gather x1, waiting for transfers between devices, shards(): lax.all_gather(up_matrix, 'sp', axis=0, tiled=True)  135 us
    all_gather x1, waiting for transfers between devices, shards(): lax.all_gather(gate_matrix, 'sp', axis=0, tiled=True)  134 us
    all_gather x2, blocking collectives, prefix(): lax.all_gather(a.astype(kind), axis)  79.8 us
    add x15, other arithmetic, join(): jnp.exp(later[0])[:, :, None] * earlier[1] + later[1]  16.1 us
  transfers between devices with their start and end apart: 6, of which 5 were waited for; matrix products, arithmetic and copies ran while one was open for 7% of the time, Pallas kernels for 0%

commit v1 on v0

--- a/solution.py
+++ b/solution.py
@@ -115,7 +115,7 @@
     gate_whole, up_whole, down_whole = (
         lax.all_gather(gate_matrix, "sp", axis=0, tiled=True),
         lax.all_gather(up_matrix, "sp", axis=0, tiled=True),
-        lax.all_gather(down_matrix, "sp", axis=1, tiled=True),
+        jnp.concatenate(lax.all_gather(down_matrix, "sp"), axis=1),
     )
     rows = query_logits.shape[0]
     head_count = extra_log_decay.shape[1]

time: 644 us -> 605 us (0.939)
  waiting for transfers between devices: 467 us -> 421 us
  local copies, waits for them, and re-layouts: 6.96 us -> 22.1 us
  other arithmetic: 36 us -> 26.3 us
    all_gather x1, waiting for transfers between devices: 183 us -> 133 us  [shards(): lax.all_gather(down_matrix, 'sp')]
    reshape x0 -> x1, local copies, waits for them, and re-layouts: none -> 15.2 us  [shards(): jnp.concatenate(lax.all_gather(down_matrix, 'sp'), axis=1)]
    all_gather x2, waiting for transfers between devices: 7.19 us -> 17.9 us  [prefix(): lax.all_gather(a.astype(kind), axis)]
    exp x15, other arithmetic: 9.83 us -> 0.17 us  [join(): jnp.exp(later[0])[:, :, None] * earlier[1] + later[1]]
    all_gather x1, waiting for transfers between devices: 134 us -> 127 us  [shards(): lax.all_gather(gate_matrix, 'sp', axis=0, tiled=True)]
  transfers between devices with their start and end apart: 6 -> 6, of which waited for: 5 -> 5; matrix products, arithmetic and copies ran while one was open for 7% -> 9% of each run, Pallas kernels for 0% -> 0%
where the time goes in v1:
time: 605 us; the launch traced here: 604 us
  waiting for transfers between devices  421 us (70%)
  blocking collectives  87.8 us (15%)
  matrix products  32.2 us (5%)
  other arithmetic  26.3 us (4%)
  local copies, waits for them, and re-layouts  22.1 us (4%)
  between operations  13.7 us (2%)
    all_gather x1, waiting for transfers between devices, shards(): lax.all_gather(up_matrix, 'sp', axis=0, tiled=True)  135 us
    all_gather x1, waiting for transfers between devices, shards(): lax.all_gather(down_matrix, 'sp')  133 us
    all_gather x1, waiting for transfers between devices, shards(): lax.all_gather(gate_matrix, 'sp', axis=0, tiled=True)  127 us
    all_gather x2, blocking collectives, prefix(): lax.all_gather(a.astype(kind), axis)  78.5 us
    all_gather x2, waiting for transfers between devices, prefix(): lax.all_gather(a.astype(kind), axis)  17.9 us
    add x15, other arithmetic, join(): jnp.exp(later[0])[:, :, None] * earlier[1] + later[1]  16.2 us
    reshape x1, local copies, waits for them, and re-layouts, shards(): jnp.concatenate(lax.all_gather(down_matrix, 'sp'), axis=1)  15.2 us
    dot_general x1, matrix products, shards(): jnp.dot(hidden, down_whole, preferred_element_type=jnp.float32)  13.8 us
  transfers between devices with their start and end apart: 6, of which 5 were waited for; matrix products, arithmetic and copies ran while one was open for 9% of the time, Pallas kernels for 0%

profile of v1, /device:TPU:0, one launch (start us, length us, event | category | flops | bytes accessed | tf_op | source)
XLA Modules:
  0.0 604.0 jit_solution(4842596748376688466)
XLA Ops:
  6.5 0.9 copy.72
  7.7 2.0 bitcast_add_fusion.1
  10.2 1.7 reshape.112
  12.0 0.8 squeeze.50
  12.7 1.0 convert_multiply_fusion.1
  13.7 0.8 squeeze.48
  14.7 2.4 exponential_multiply_fusion.3
  17.1 1.3 fusion.7
  18.5 2.0 fusion.6
  20.6 0.7 all-gather.17.cloned.1.call-update
  22.5 42.6 %all_gather.41 = bf16[16,4,128]{2,1,0:T(4,128)(2,1)S(1)} all-gather(bf16[1,4,128]{2,1,0:T(4,128)(2,1)S(1)} %slice.20), channel_id=1, replica_groups=mesh['sp'=16,'tp'=2] {'sp'}, dimensions={0}, use_global_device_ids=true | all-gather | bytes 17408 | tf_op jit(solution)/shard_map/all_gather | solution.py:19
  65.1 35.8 %all_gather.38 = bf16[16,4,128]{2,1,0:T(4,128)(2,1)S(1)} all-gather(bf16[1,4,128]{2,1,0:T(4,128)(2,1)S(1)} %slice.21), channel_id=1, replica_groups=mesh['sp'=16,'tp'=2] {'sp'}, dimensions={0}, use_global_device_ids=true | all-gather | bytes 17408 | tf_op jit(solution)/shard_map/all_gather | solution.py:19
  101.0 1.6 convolution_multiply_fusion.2
  103.7 0.7 convolution_multiply_fusion.1
  105.7 17.0 %while.17 = (s32[]{:T(128)}, f32[4,128,128]{2,1,0:T(8,128)S(1)}, s32[]{:T(128)}, bf16[16,4,128]{2,1,0:T(4,128)(2,1)S(1)}, bf16[16,4,128,128]{3,2,1,0:T(8,128)(2,...) while((s32[]{:T(128)}, f32[4,128,128]{2,1,0:T(8,128)S(1)}, s32[]{:T(128)}, ...), condition=%wide.region_5.6_spmd, body=%wide.region_4.5_spmd.sunk | while | flops 197126 | bytes 660627 | solution.py:34
  105.7 1.1 convert_add_fusion.6
  106.9 1.1 convert_add_fusion.6
  108.0 1.1 convert_add_fusion.6
  109.2 1.1 convert_add_fusion.6
  110.3 1.1 convert_add_fusion.6
  111.4 1.1 convert_add_fusion.6
  112.5 1.1 convert_add_fusion.6
  113.7 1.1 convert_add_fusion.6
  114.8 1.1 convert_add_fusion.6
  115.9 1.1 convert_add_fusion.6
  117.0 1.1 convert_add_fusion.6
  118.2 1.1 convert_add_fusion.6
  119.3 1.1 convert_add_fusion.6
  120.4 1.1 convert_add_fusion.6
  121.6 1.1 convert_add_fusion.6
  122.7 1.3 fusion.1
  124.0 1.9 rev.20
  125.9 17.9 %all-gather.13.cloned.1.call-done = bf16[64,128,128]{2,1,0:T(8,128)(2,1)} async-done(((bf16[4,128,128]{2,1,0:T(8,128)(2,1)}), bf16[64,128,128]{2,1,0:T(8,128)(2,1)}) %all-gather.13.cloned.1.call-update) | async-done | bytes 2097168 | tf_op jit(solution)/shard_map/all_gather | solution.py:19
  144.5 0.7 multiply_multiply_fusion
  145.5 2.0 all_gather.44
  147.5 1.5 fusion.37
  149.0 2.5 all-reduce.1
  151.7 2.4 all_gather.45
  154.1 132.8 %all-gather.17.cloned.1.call-done = bf16[45056,128]{1,0:T(8,128)(2,1)} async-done(((bf16[2816,128]{1,0:T(8,128)(2,1)}), bf16[45056,128]{1,0:T(8,128)(2,1)}) %all-gather.17.cloned.1.call-update) | async-done | bytes 11534352 | tf_op jit(solution)/shard_map/all_gather | solution.py:118
  286.8 15.2 %copy.92 = bf16[2816,16,128]{0,2,1:T(8,128)(2,1)} copy(bf16[2816,16,128]{2,0,1:T(8,128)(2,1)} %bitcast.89) | data formatting | bytes 23068672 | tf_op jit(solution)/shard_map/reshape | solution.py:118
  302.0 127.1 %all-gather.9.cloned.1.call-done = bf16[2048,2816]{1,0:T(8,128)(2,1)} async-done(((bf16[128,2816]{1,0:T(8,128)(2,1)}), bf16[2048,2816]{1,0:T(8,128)(2,1)}) %all-gather.9.cloned.1.call-update) | async-done | bytes 11534352 | tf_op jit(solution)/shard_map/all_gather | solution.py:116
  429.1 7.1 %fusion.40 = f32[128,2816]{1,0:T(8,128)} fusion(bf16[128,2048]{1,0:T(8,128)(2,1)S(1)} %all_gather.45, bf16[2048,2816]{1,0:T(8,128)(2,1)} %all-gather.9.cloned.1.call-done), kind=kOutput, calls=%fused_computation.91 | convolution fusion | flops 1476395008 | bytes 13500416 | tf_op jit(solution)/shard_map/dot_general | solution.py:179
  436.2 135.2 %all-gather.11.cloned.1.call-done = bf16[2048,2816]{1,0:T(8,128)(2,1)} async-done(((bf16[128,2816]{1,0:T(8,128)(2,1)}), bf16[2048,2816]{1,0:T(8,128)(2,1)}) %all-gather.11.cloned.1.call-update) | async-done | bytes 11534352 | tf_op jit(solution)/shard_map/all_gather | solution.py:117
  571.3 13.8 %convolution_convert_fusion = bf16[128,2048]{1,0:T(8,128)(2,1)} fusion(bf16[2816,2048]{0,1:T(8,128)(2,1)} %bitcast.90, bf16[128,2048]{1,0:T(8,128)(2,1)S(1)} %all_gather.45, bf16[2048,2816]{1,0:T(8,128)(2,1)} %all-gather.11.cloned.1.call-done, f32[128,2816]{1,0:T(8,128)} %fusion.40), kind=kOutput, calls=%fused_computation.6 | convolution fusion | flops 2955214848 | bytes 25559040 | tf_op jit(solution)/shard_map/dot_general | solution.py:182
  585.2 6.3 %reduce-scatter.2.cloned.1.call-done = bf16[128,1024]{1,0:T(8,128)(2,1)} async-done(((bf16[128,2048]{1,0:T(8,128)(2,1)}), bf16[128,1024]{1,0:T(8,128)(2,1)}) %reduce-scatter.2.cloned.1.call-update) | async-done | bytes 262160 | tf_op jit(solution)/shard_map/reduce_scatter | solution.py:183
  591.4 1.3 fusion.8
  592.7 2.5 all-reduce
  595.2 1.9 add_convert_fusion
  (73 shorter events, 5.8 us)
Async XLA Ops:
  6.5 141.0 %copy-start = (bf16[1024,1024]{1,0:T(8,128)(2,1)S(1)}, bf16[1024,1024]{1,0:T(8,128)(2,1)}, u32[]{:S(2)}) copy-start(bf16[1024,1024]{1,0:T(8,128)(2,1)} %param.32) | copy-start | bytes 6291460
  6.5 99.1 %all-gather.15.cloned.1.call-start = ((), (), s32[]{:S(2)}) async-start(), calls=%async_computation.5 | async-start | bytes 2228224 | tf_op jit(solution)/shard_map/all_gather | solution.py:19
  9.8 4.8 copy-start.2
  18.4 125.4 %all-gather.13.cloned.1.call-start = ((), (), s32[]{:S(2)}) async-start(), calls=%async_computation.4 | async-start | bytes 2228224 | tf_op jit(solution)/shard_map/all_gather | solution.py:19
  20.5 266.3 %all-gather.17.cloned.1.call-start = ((), (), s32[]{:S(2)}) async-start(), calls=%async_computation.6 | async-start | bytes 12255232 | tf_op jit(solution)/shard_map/all_gather | solution.py:118
  21.3 407.8 %all-gather.9.cloned.1.call-start = ((), (), s32[]{:S(2)}) async-start(), calls=%async_computation.1 | async-start | bytes 12255232 | tf_op jit(solution)/shard_map/all_gather | solution.py:116
  21.8 549.5 %all-gather.11.cloned.1.call-start = ((), (), s32[]{:S(2)}) async-start(), calls=%async_computation.2 | async-start | bytes 12255232 | tf_op jit(solution)/shard_map/all_gather | solution.py:117
  22.4 569.0 %reduce-scatter.2.cloned.1.call-start = ((), (), s32[]{:S(2)}) async-start(), calls=%async_computation.3 | async-start | bytes 786432 | tf_op jit(solution)/shard_map/reduce_scatter | solution.py:183
  22.5 81.2 %copy-start.3 = (f32[128,4,128]{2,1,0:T(4,128)S(1)}, f32[128,4,128]{2,1,0:T(4,128)}, u32[]{:S(2)}) copy-start(f32[128,4,128]{2,1,0:T(4,128)} %get-tuple-element.229) | copy-start | bytes 786436
  143.8 1.6 copy-start.4
  145.4 6.1 %copy-start.5 = (f32[1024]{0:T(1024)S(1)}, f32[1024]{0:T(1024)}, u32[]{:S(2)}) copy-start(f32[1024]{0:T(1024)} %param.34) | copy-start | bytes 12292
  145.4 6.1 %copy-start.6 = (f32[1024]{0:T(1024)S(1)}, f32[1024]{0:T(1024)}, u32[]{:S(2)}) copy-start(f32[1024]{0:T(1024)} %param.33) | copy-start | bytes 12292
  571.3 23.8 %copy-start.7 = (f32[1024]{0:T(1024)S(1)}, f32[1024]{0:T(1024)}, u32[]{:S(2)}) copy-start(f32[1024]{0:T(1024)} %param.39) | copy-start | bytes 12292
  571.3 23.8 %copy-start.8 = (f32[1024]{0:T(1024)S(1)}, f32[1024]{0:T(1024)}, u32[]{:S(2)}) copy-start(f32[1024]{0:T(1024)} %param.38) | copy-start | bytes 12292
  571.3 25.8 %copy-start.1 = (bf16[1024,1024]{1,0:T(8,128)(2,1)S(1)}, bf16[1024,1024]{1,0:T(8,128)(2,1)}, u32[]{:S(2)}) copy-start(bf16[1024,1024]{1,0:T(8,128)(2,1)} %param.32) | copy-start | bytes 6291460
Sparse Core Ops, SparseCore 0:
  18.5 63.2 all-gather.14
  84.6 59.1 all-gather.12
  146.6 140.2 all-gather.16
  289.5 139.5 all-gather.8
  431.7 139.5 all-gather.10
  585.3 6.0 reduce-scatter.1
